TPU v7x, 32 devices: a whole 2x2x4 slice. The times are simulated.
32 devices in a mesh: fs: 4 (over z), rep: 4 (over y, x), tp: 2 (over core).
Axes of the slice: x: 2, y: 2, z: 4, core: 2. Of those that a mesh axis runs over, the one named last changes fastest.
Arguments:
- inputs: bfloat16 [2048, 2048], P(('fs', 'rep')), may hold values from -6 to 6
- query_cot: bfloat16 [2048, 1024], P(('fs', 'rep'), 'tp'), may hold values from -0.125 to 0.125
- attended: bfloat16 [2048, 1024], P(('fs', 'rep')), may hold values from -6 to 6
- output_cot: bfloat16 [2048, 2048], P(('fs', 'rep'), 'tp'), may hold values from -0.125 to 0.125
- proj_query: bfloat16 [2048, 256], P('fs'), may hold values from -0.125 to 0.125
- proj_output: bfloat16 [1024, 256], P('fs'), may hold values from -0.1875 to 0.1875
- weight_query: float32 [2048, 1024], P('fs', 'tp'), may hold values from -0.125 to 0.125
- weight_output: float32 [1024, 2048], P('fs', 'tp'), may hold values from -0.1875 to 0.1875
- first_query: float32 [256, 1024], P('fs', 'tp'), may hold values from -6 to 6
- second_query: float32 [256, 1024], P('fs', 'tp'), may hold values from 0.0002 to 2
- first_output: float32 [256, 2048], P('fs', 'tp'), may hold values from -6 to 6
- second_output: float32 [256, 2048], P('fs', 'tp'), may hold values from 0.0002 to 2
Outputs:
- new_weight_query: float32 [2048, 1024], P('fs', 'tp')
- new_weight_output: float32 [1024, 2048], P('fs', 'tp')
- step_query: float32 [2048, 1024], P('fs', 'tp')
- step_output: float32 [1024, 2048], P('fs', 'tp')
- new_first_query: float32 [256, 1024], P('fs', 'tp')
- new_second_query: float32 [256, 1024], P('fs', 'tp')
- new_first_output: float32 [256, 2048], P('fs', 'tp')
- new_second_output: float32 [256, 2048], P('fs', 'tp')
- copy_query: bfloat16 [2048, 1024], P(None, 'tp')
- copy_output: bfloat16 [1024, 2048], P(None, 'tp')
All inputs are finite; a program needn't handle non-finite values.
Results may differ from a plain program's by a relative error of at most 0.0031.
Values may be sent and summed in bfloat16 or wider, within the bound.
A program may use at most 64 MiB of HBM per device.

v0:
```python
import jax
import jax.numpy as jnp
from jax import lax
from jax.sharding import PartitionSpec as P

D = 2048
DA = 1024
RANK = 256


beta_first = 0.9
beta_second = 0.95
adam_eps = 1e-08
mean_eps = 1e-06
learn_rate = 0.02


def contract_rows(left, right):
    return lax.dot_general(
        left,
        right,
        (((0,), (0,)), ((), ())),
        precision=lax.Precision.HIGHEST,
        preferred_element_type=jnp.float32,
    )


def moment_update(low_sum, first, second):
    first_new = beta_first * first + (1.0 - beta_first) * low_sum
    second_new = beta_second * second + (1.0 - beta_second) * low_sum * low_sum
    normed = first_new / (jnp.sqrt(second_new) + adam_eps)
    return (first_new, second_new, normed)


def local(
    inputs,
    query_cot,
    attended,
    output_cot,
    proj_query,
    proj_output,
    weight_query,
    weight_output,
    first_query,
    second_query,
    first_output,
    second_output,
):
    whole_query, whole_output = (
        lax.all_gather(proj_query, "fs", axis=0, tiled=True),
        lax.all_gather(proj_output, "fs", axis=0, tiled=True),
    )
    reduced_query = jnp.dot(inputs, whole_query, preferred_element_type=jnp.float32)
    reduced_output = jnp.dot(attended, whole_output, preferred_element_type=jnp.float32)
    part_query = contract_rows(reduced_query, query_cot.astype(jnp.float32))
    part_output = contract_rows(reduced_output, output_cot.astype(jnp.float32))
    low_query, low_output = (
        lax.psum_scatter(part_query, "fs", scatter_dimension=0, tiled=True),
        lax.psum_scatter(part_output, "fs", scatter_dimension=0, tiled=True),
    )
    low_query, low_output = lax.psum((low_query, low_output), "rep")
    first_q, second_q, normed_q = moment_update(low_query, first_query, second_query)
    first_o, second_o, normed_o = moment_update(low_output, first_output, second_output)
    local_total = jnp.sum(normed_q * normed_q) + jnp.sum(normed_o * normed_o)
    total = lax.psum(local_total, ("fs", "tp"))
    scale = lax.rsqrt(total / (RANK * (DA + D)) + mean_eps)
    half_q = normed_q.astype(jnp.bfloat16)
    half_o = normed_o.astype(jnp.bfloat16)
    update_query = jnp.dot(
        proj_query,
        lax.all_gather(half_q, "fs", axis=0, tiled=True),
        preferred_element_type=jnp.float32,
    )
    update_output = jnp.dot(
        proj_output,
        lax.all_gather(half_o, "fs", axis=0, tiled=True),
        preferred_element_type=jnp.float32,
    )
    step_q = scale * update_query
    step_o = scale * update_output
    new_q = weight_query - learn_rate * step_q
    new_o = weight_output - learn_rate * step_o
    copy_q, copy_o = (
        lax.all_gather(new_q.astype(jnp.bfloat16), "fs", axis=0, tiled=True),
        lax.all_gather(new_o.astype(jnp.bfloat16), "fs", axis=0, tiled=True),
    )
    return (new_q, new_o, step_q, step_o, first_q, second_q, first_o, second_o, copy_q, copy_o)


def solution(mesh):
    return jax.shard_map(
        local,
        mesh=mesh,
        in_specs=(
            P(("fs", "rep"), None),
            P(("fs", "rep"), "tp"),
            P(("fs", "rep"), None),
            P(("fs", "rep"), "tp"),
            P("fs", None),
            P("fs", None),
            P("fs", "tp"),
            P("fs", "tp"),
            P("fs", "tp"),
            P("fs", "tp"),
            P("fs", "tp"),
            P("fs", "tp"),
        ),
        out_specs=(
            P("fs", "tp"),
            P("fs", "tp"),
            P("fs", "tp"),
            P("fs", "tp"),
            P("fs", "tp"),
            P("fs", "tp"),
            P("fs", "tp"),
            P("fs", "tp"),
            P(None, "tp"),
            P(None, "tp"),
        ),
        check_vma=False,
    )
```

profile of v0, /device:TPU:27, one launch (start us, length us, event | category | flops | bytes accessed | tf_op | source)
XLA Modules:
  0.0 280.9 jit_solution(2093168911160044826)
XLA Ops:
  7.2 0.0 copy-start
  7.2 0.0 all-gather.4.cloned.1.call-start
  7.2 0.7 all-gather.4.cloned.1.call-update
  7.9 0.0 reduce-scatter.5.cloned.1.call-start
  8.0 13.4 %all_gather.19 = bf16[1024,256]{1,0:T(8,128)(2,1)S(1)} all-gather(bf16[256,256]{1,0:T(8,128)(2,1)} %param.17), channel_id=1, replica_groups=mesh['fs'=4,'rep'=4,'tp'=2] {'fs'}, dimensions={0}, use_global_device_ids=true | all-gather | bytes 655360 | tf_op jit(solution)/shard_map/all_gather | solution.py:51
  21.3 1.2 fusion.12
  22.5 0.0 copy-start.11
  22.6 2.6 fusion.13
  25.1 0.0 copy-start.9
  25.1 0.0 copy-start.10
  25.1 0.0 reduce-scatter.5.cloned.1.call-update
  25.2 0.0 reduce-scatter.3.cloned.1.call-start
  25.2 13.5 %all-gather.4.cloned.1.call-done = bf16[2048,256]{1,0:T(8,128)(2,1)} async-done(((bf16[512,256]{1,0:T(8,128)(2,1)}), bf16[2048,256]{1,0:T(8,128)(2,1)}) %all-gather.4.cloned.1.call-update) | async-done | bytes 1048592 | tf_op jit(solution)/shard_map/all_gather | solution.py:50
  38.7 0.0 copy-done
  38.7 1.5 fusion.10
  40.2 0.0 copy-done.11
  40.2 0.0 copy-start.12
  40.2 0.0 copy-start.13
  40.3 0.0 copy-start.3
  40.3 1.2 fusion.11
  41.5 0.0 reduce-scatter.3.cloned.1.call-update
  41.5 0.0 all-reduce.3.cloned.1.call-start
  41.6 25.4 %reduce-scatter.5.cloned.1.call-done = f32[64,1024]{1,0:T(8,128)} async-done(((f32[256,1024]{1,0:T(8,128)}), f32[64,1024]{1,0:T(8,128)}) %reduce-scatter.5.cloned.1.call-update) | async-done | bytes 262160 | tf_op jit(solution)/shard_map/reduce_scatter | solution.py:59
  66.9 22.1 %reduce-scatter.3.cloned.1.call-done = f32[64,512]{1,0:T(8,128)} async-done(((f32[256,512]{1,0:T(8,128)}), f32[64,512]{1,0:T(8,128)}) %reduce-scatter.3.cloned.1.call-update) | async-done | bytes 131088 | tf_op jit(solution)/shard_map/reduce_scatter | solution.py:58
  89.1 0.0 all-reduce.3.cloned.1.call-update
  89.1 0.0 all-gather.8.cloned.1.call-start
  89.1 48.7 %all-reduce.3.cloned.1.call-done = (f32[64,512]{1,0:T(8,128)}, f32[64,1024]{1,0:T(8,128)}) async-done(((f32[64,512]{1,0:T(8,128)}, f32[64,1024]{1,0:T(8,128)}), (f32[64,512]{1,0:T(8,128)}, f32[64,1024]{1,0:T(8,128)})) %all-reduce.3.cloned.1.call-update) | async-done | bytes 393232 | tf_op jit(solution)/shard_map/psum | solution.py:61
  137.9 0.0 copy-done.9
  137.9 0.0 copy-done.10
  137.9 1.1 fusion.5
  139.0 0.0 copy-start.4
  139.0 0.0 copy-start.5
  139.0 0.0 copy-start.6
  139.0 0.7 multiply_reduce_fusion
  139.7 0.0 copy-done.12
  139.7 0.0 copy-done.13
  139.8 2.2 multiply_reduce_fusion.1
  143.3 0.0 copy-done.3
  143.3 1.3 copy.23
  144.6 13.5 %psum.23 = f32[]{:T(128)} all-reduce(f32[]{:T(128)S(6)} %add.48), channel_id=1, replica_groups=mesh['fs'=4,'rep'=4,'tp'=2] {'fs','tp'}, use_global_device_ids=true, to_apply=%region_6.0 | all-reduce | flops 1 | bytes 8 | tf_op jit(solution)/shard_map/psum | solution.py:65
  158.8 14.0 %all_gather.21 = bf16[256,1024]{1,0:T(8,128)(2,1)S(1)} all-gather(bf16[64,1024]{1,0:T(8,128)(2,1)S(1)} %get-tuple-element.26), channel_id=1, replica_groups=mesh['fs'=4,'rep'=4,'tp'=2] {'fs'}, dimensions={0}, use_global_device_ids=true | all-gather | bytes 655360 | tf_op jit(solution)/shard_map/all_gather | solution.py:76
  172.8 0.0 copy-done.6
  172.8 2.4 fusion.6
  175.2 0.0 copy-done.4
  175.2 0.0 copy-done.5
  175.2 0.0 all-gather.8.cloned.1.call-update
  175.3 0.0 all-gather.6.cloned.1.call-start
  175.3 2.6 copy.22
  177.9 0.0 copy-done.7
  177.9 0.0 copy-done.8
  177.9 0.1 fusion.4
  177.9 12.4 %all_gather.20 = bf16[256,512]{1,0:T(8,128)(2,1)S(1)} all-gather(bf16[64,512]{1,0:T(8,128)(2,1)S(1)} %fusion.4), channel_id=1, replica_groups=mesh['fs'=4,'rep'=4,'tp'=2] {'fs'}, dimensions={0}, use_global_device_ids=true | all-gather | bytes 327680 | tf_op jit(solution)/shard_map/all_gather | solution.py:71
  190.3 0.0 copy-done.2
  190.3 3.1 %fusion.7 = (bf16[512,512]{0,1:T(8,128)(2,1)}, f32[512,512]{0,1:T(8,128)}, f32[512,512]{0,1:T(8,128)}) fusion(f32[512,512]{0,1:T(8,128)} %copy.22, bf16[256,512]{1,0:T(8,128)(2,1)S(1)} %all_gather.20, bf16[512,256]{1,0:T(8,128)(2,1)S(1)} %copy-done.2, f32[]{:T(128)S(6)} %rsqrt.3), kind=kOutput, calls=%fused_computation.19 | convolution fusion | flops 135266304 | bytes 4194308 | tf_op jit(solution)/shard_map/dot_general | solution.py:69
  193.4 0.0 all-gather.6.cloned.1.call-update
  193.5 1.3 copy.25
  194.8 1.3 copy.27
  196.1 2.5 copy.24
  198.6 0.0 copy-done.1
  198.6 1.3 copy.26
  199.9 24.2 %all-gather.8.cloned.1.call-done = bf16[1024,1024]{0,1:T(8,128)(2,1)} async-done(((bf16[256,1024]{0,1:T(8,128)(2,1)}), bf16[1024,1024]{0,1:T(8,128)(2,1)}) %all-gather.8.cloned.1.call-update) | async-done | bytes 2097168 | tf_op jit(solution)/shard_map/all_gather | solution.py:85
  224.2 3.9 %copy.29 = bf16[1024,1024]{1,0:T(8,128)(2,1)} copy(bf16[1024,1024]{0,1:T(8,128)(2,1)} %all-gather.8.cloned.1.call-done) | data formatting | bytes 4194304
  228.1 42.0 %all-gather.6.cloned.1.call-done = bf16[2048,512]{0,1:T(8,128)(2,1)} async-done(((bf16[512,512]{0,1:T(8,128)(2,1)}), bf16[2048,512]{0,1:T(8,128)(2,1)}) %all-gather.6.cloned.1.call-update) | async-done | bytes 2097168 | tf_op jit(solution)/shard_map/all_gather | solution.py:84
  270.1 3.9 %copy.28 = bf16[2048,512]{1,0:T(8,128)(2,1)} copy(bf16[2048,512]{0,1:T(8,128)(2,1)} %all-gather.6.cloned.1.call-done) | data formatting | bytes 4194304
  (4 shorter events, 0.0 us)
Async XLA Ops:
  7.2 31.5 %copy-start = (bf16[128,2048]{1,0:T(8,128)(2,1)S(1)}, bf16[128,2048]{1,0:T(8,128)(2,1)}, u32[]{:S(2)}) copy-start(bf16[128,2048]{1,0:T(8,128)(2,1)} %param.12) | copy-start | bytes 1572868
  7.2 31.5 %all-gather.4.cloned.1.call-start = ((), (), s32[]{:S(2)}) async-start(), calls=%async_computation.2 | async-start | bytes 1310720 | tf_op jit(solution)/shard_map/all_gather | solution.py:50
  7.9 59.0 %reduce-scatter.5.cloned.1.call-start = ((), (), s32[]{:S(2)}) async-start(), calls=%async_computation.4 | async-start | bytes 1310720 | tf_op jit(solution)/shard_map/reduce_scatter | solution.py:59
  22.5 17.7 %copy-start.11 = (bf16[128,512]{1,0:T(8,128)(2,1)S(1)}, bf16[128,512]{1,0:T(8,128)(2,1)}, u32[]{:S(2)}) copy-start(bf16[128,512]{1,0:T(8,128)(2,1)} %param.13) | copy-start | bytes 393220
  25.1 112.8 %copy-start.9 = (f32[64,1024]{1,0:T(8,128)S(1)}, f32[64,1024]{1,0:T(8,128)}, u32[]{:S(2)}) copy-start(f32[64,1024]{1,0:T(8,128)} %param.23) | copy-start | bytes 786436
  25.1 112.8 %copy-start.10 = (f32[64,1024]{1,0:T(8,128)S(1)}, f32[64,1024]{1,0:T(8,128)}, u32[]{:S(2)}) copy-start(f32[64,1024]{1,0:T(8,128)} %param.22) | copy-start | bytes 786436
  25.2 63.9 %reduce-scatter.3.cloned.1.call-start = ((), (), s32[]{:S(2)}) async-start(), calls=%async_computation.3 | async-start | bytes 655360 | tf_op jit(solution)/shard_map/reduce_scatter | solution.py:58
  40.2 99.5 %copy-start.12 = (f32[64,512]{1,0:T(8,128)S(1)}, f32[64,512]{1,0:T(8,128)}, u32[]{:S(2)}) copy-start(f32[64,512]{1,0:T(8,128)} %param.21) | copy-start | bytes 393220
  40.2 99.5 %copy-start.13 = (f32[64,512]{1,0:T(8,128)S(1)}, f32[64,512]{1,0:T(8,128)}, u32[]{:S(2)}) copy-start(f32[64,512]{1,0:T(8,128)} %param.20) | copy-start | bytes 393220
  40.3 103.0 %copy-start.3 = (f32[256,1024]{1,0:T(8,128)S(1)}, f32[256,1024]{1,0:T(8,128)}, u32[]{:S(2)}) copy-start(f32[256,1024]{1,0:T(8,128)} %param.19) | copy-start | bytes 3145732
  41.5 96.4 %all-reduce.3.cloned.1.call-start = ((), (), s32[]{:S(2)}) async-start(), calls=%async_computation.7 | async-start | bytes 786432 | tf_op jit(solution)/shard_map/psum | solution.py:61
  89.1 135.1 %all-gather.8.cloned.1.call-start = ((), (), s32[]{:S(2)}) async-start(), calls=%async_computation.6 | async-start | bytes 2621440 | tf_op jit(solution)/shard_map/all_gather | solution.py:85
  139.0 36.2 %copy-start.4 = (f32[64,1024]{1,0:T(8,128)}, f32[64,1024]{1,0:T(8,128)S(1)}, u32[]{:S(2)}) copy-start(f32[64,1024]{1,0:T(8,128)S(1)} %get-tuple-element.27) | copy-start | bytes 786436
  139.0 36.2 %copy-start.5 = (f32[64,1024]{1,0:T(8,128)}, f32[64,1024]{1,0:T(8,128)S(1)}, u32[]{:S(2)}) copy-start(f32[64,1024]{1,0:T(8,128)S(1)} %get-tuple-element.28) | copy-start | bytes 786436
  139.0 33.8 %copy-start.6 = (bf16[256,256]{1,0:T(8,128)(2,1)S(1)}, bf16[256,256]{1,0:T(8,128)(2,1)}, u32[]{:S(2)}) copy-start(bf16[256,256]{1,0:T(8,128)(2,1)} %param.17) | copy-start | bytes 393220
  142.0 35.9 %copy-start.7 = (f32[64,512]{1,0:T(8,128)}, f32[64,512]{1,0:T(8,128)S(1)}, u32[]{:S(2)}) copy-start(f32[64,512]{1,0:T(8,128)S(1)} %get-tuple-element.30) | copy-start | bytes 393220
  175.2 15.1 %copy-start.2 = (bf16[512,256]{1,0:T(8,128)(2,1)S(1)}, bf16[512,256]{1,0:T(8,128)(2,1)}, u32[]{:S(2)}) copy-start(bf16[512,256]{1,0:T(8,128)(2,1)} %param.16) | copy-start | bytes 786436
  175.2 2.7 copy-start.8
  175.3 94.8 %all-gather.6.cloned.1.call-start = ((), (), s32[]{:S(2)}) async-start(), calls=%async_computation.5 | async-start | bytes 2621440 | tf_op jit(solution)/shard_map/all_gather | solution.py:84
  194.8 3.9 %copy-start.1 = (f32[512,512]{0,1:T(8,128)S(1)}, f32[512,512]{0,1:T(8,128)}, u32[]{:S(2)}) copy-start(f32[512,512]{0,1:T(8,128)} %get-tuple-element.32) | copy-start | bytes 3145732
Sparse Core Ops, SparseCore 0:
  9.6 29.0 all-gather.3
  41.5 25.3 reduce-scatter.4
  69.8 19.2 reduce-scatter.2
  91.9 45.9 all-reduce.2
  175.4 48.7 all-gather.7
  226.2 43.8 all-gather.5
where the time goes:
time: 285 us; the launch traced here: 281 us
  waiting for transfers between devices  177 us (62%)
  blocking collectives  53.3 us (19%)
  local copies, waits for them, and re-layouts  18.3 us (6%)
  between operations  16.2 us (6%)
  matrix products  12 us (4%)
  other arithmetic  4.11 us (1%)
    psum x1, waiting for transfers between devices, local(): low_query, low_output = lax.psum((low_query, low_output), 'rep')  48.7 us
    all_gather x1, waiting for transfers between devices, local(): lax.all_gather(new_q.astype(jnp.bfloat16), 'fs', axis=0, tiled=True)  42 us
    reduce_scatter x1, waiting for transfers between devices, local(): lax.psum_scatter(part_output, 'fs', scatter_dimension=0, tiled=True)  25.4 us
    all_gather x1, waiting for transfers between devices, local(): lax.all_gather(new_o.astype(jnp.bfloat16), 'fs', axis=0, tiled=True)  24.2 us
    reduce_scatter x1, waiting for transfers between devices, local(): lax.psum_scatter(part_query, 'fs', scatter_dimension=0, tiled=True)  22.1 us
    unnamed x36, local copies, waits for them, and re-layouts  18.3 us
    all_gather x1, blocking collectives, local(): lax.all_gather(half_o, 'fs', axis=0, tiled=True)  14 us
    psum x1, blocking collectives, local(): total = lax.psum(local_total, ('fs', 'tp'))  13.5 us
  transfers between devices with their start and end apart: 6, of which 6 were waited for; matrix products, arithmetic and copies ran while one was open for 8% of the time, Pallas kernels for 0%

commit v1 on v0

v1 whole, which is shorter than its diff:
```python
import functools

import jax
import jax.numpy as jnp
from jax import lax
from jax.experimental import pallas as pl
from jax.experimental.pallas import tpu as pltpu
from jax.sharding import PartitionSpec as P

beta_first = 0.9
beta_second = 0.95
adam_eps = 1e-08
mean_eps = 1e-06
learn_rate = 0.02

MESH = pl.DeviceIdType.MESH
F32 = jnp.float32
BF16 = jnp.bfloat16


def kernel(
    n, r, tp, entries,
    x_ref, qc_ref, a_ref, oc_ref, pq_ref, po_ref, wq_ref, wo_ref, fq_ref, sq_ref, fo_ref, so_ref,
    nwq, nwo, stq, sto, nfq, nsq, nfo, nso, cpq, cpo,
    allq, allo, allx, alla, allqc, alloc, sbuf, r2, lowg, half, tz, tr, tt,
    pz_s, pz_r, pt_s, pt_r, xr_s, xr_r, xt_s, xt_r, cr1_s, cr1_r, r2_s, r2_r, lg_s, lg_r, hz_s, hz_r, hr_s, hr_r,
    tz_s, tz_r, tr_s, tr_r, tt_s, tt_r, cz_s, cz_r, cr_s, cr_r,
):
    f, k, t = lax.axis_index("fs"), lax.axis_index("rep"), lax.axis_index("tp")
    other = {"tp": 1 - t}
    rows_q, rank = pq_ref.shape
    rows_o = po_ref.shape[0]
    low_rows = fq_ref.shape[0]
    quarter_q, quarter_o = fq_ref.shape[1] // r, fo_ref.shape[1] // r
    fs_peers = [lax.rem(f + d, n) for d in range(1, n)]
    rep_peers = [lax.rem(k + d, r) for d in range(1, r)]

    def send(src, dst, ssem, rsem, where):
        copy = pltpu.make_async_remote_copy(
            src_ref=src, dst_ref=dst, send_sem=ssem, recv_sem=rsem, device_id=where, device_id_type=MESH
        )
        copy.start()
        return copy

    def arrived(dst, ssem, rsem, where):
        pltpu.make_async_remote_copy(
            src_ref=dst, dst_ref=dst, send_sem=ssem, recv_sem=rsem, device_id=where, device_id_type=MESH
        ).wait_recv()

    def cols(index, width):
        return pl.ds(pl.multiple_of(index * width, width), width)

    barrier = pltpu.get_barrier_semaphore()
    for j in fs_peers:
        pl.semaphore_signal(barrier, inc=1, device_id={"fs": j}, device_id_type=MESH)
    for j in rep_peers:
        pl.semaphore_signal(barrier, inc=1, device_id={"rep": j}, device_id_type=MESH)
    pl.semaphore_signal(barrier, inc=1, device_id=other, device_id_type=MESH)
    pl.semaphore_wait(barrier, n - 1 + r - 1 + 1)

    sent = []
    tokens = x_ref.shape[0]
    pieces = ((pq_ref, allq, rows_q // tp, 0), (po_ref, allo, rows_o // tp, 1))
    loads = ((x_ref, allx, tokens // tp, 0), (a_ref, alla, tokens // tp, 1))
    for j in fs_peers:
        for own, whole, part, i in pieces:
            mine = cols(t, part)
            sent.append(send(own.at[mine], whole.at[f, mine], pz_s.at[i, j], pz_r.at[i, f], {"fs": j}))
    for j in rep_peers:
        for own, whole, part, i in loads:
            mine = cols(t, part)
            sent.append(send(own.at[mine], whole.at[k, mine], xr_s.at[i, j], xr_r.at[i, k], {"rep": j}))
    for j in rep_peers:
        for own, whole, width, i in ((qc_ref, allqc, quarter_q, 0), (oc_ref, alloc, quarter_o, 1)):
            sent.append(send(own.at[:, cols(j, width)], whole.at[k], cr1_s.at[i, j], cr1_r.at[i, k], {"rep": j}))
    allq[f] = pq_ref[...]
    allo[f] = po_ref[...]
    allx[k] = x_ref[...]
    alla[k] = a_ref[...]
    allqc[k] = qc_ref[:, cols(k, quarter_q)]
    alloc[k] = oc_ref[:, cols(k, quarter_o)]
    for d in range(max(n, r) - 1):
        for peers, group, s1, r1, s2, r2_, axis in (
            (fs_peers, pieces, pz_s, pz_r, pt_s, pt_r, "fs"),
            (rep_peers, loads, xr_s, xr_r, xt_s, xt_r, "rep"),
        ):
            if d >= len(peers):
                continue
            j = peers[d]
            for own, whole, part, i in group:
                mine = cols(t, part)
                arrived(whole.at[j, mine], s1.at[i, j], r1.at[i, j], {axis: j})
                sent.append(send(whole.at[j, mine], whole.at[j, mine], s2.at[i, j], r2_.at[i, j], other))
    for peers, group, s2, r2_ in ((fs_peers, pieces, pt_s, pt_r), (rep_peers, loads, xt_s, xt_r)):
        for j in peers:
            for own, whole, part, i in group:
                arrived(whole.at[j, cols(1 - t, part)], s2.at[i, j], r2_.at[i, j], other)
    for j in rep_peers:
        for whole, i in ((allqc, 0), (alloc, 1)):
            arrived(whole.at[j], cr1_s.at[i, j], cr1_r.at[i, j], {"rep": j})

    def projected(load, factor, cot):
        load, factor, cot = (v[...].reshape(-1, v.shape[-1]) for v in (load, factor, cot))
        turned = jnp.dot(load, factor, preferred_element_type=F32).T
        high = turned.astype(BF16)
        rest = (turned - high.astype(F32)).astype(BF16)
        return jnp.dot(high, cot, preferred_element_type=F32) + jnp.dot(rest, cot, preferred_element_type=F32)

    total_q = projected(allx, allq, allqc)
    total_o = projected(alla, allo, alloc)
    sbuf[:, :, :quarter_q] = total_q.reshape(n, low_rows, quarter_q)
    sbuf[:, :, quarter_q:] = total_o.reshape(n, low_rows, quarter_o)
    for j in fs_peers:
        sent.append(send(sbuf.at[j], r2.at[f], r2_s.at[j], r2_r.at[f], {"fs": j}))
    low = sbuf[f]
    for j in fs_peers:
        arrived(r2.at[j], r2_s.at[j], r2_r.at[j], {"fs": j})
        low += r2[j]
    lowg[k] = low

    def update(low_sum, first, second):
        first_new = beta_first * first + (1.0 - beta_first) * low_sum
        second_new = beta_second * second + (1.0 - beta_second) * low_sum * low_sum
        return first_new, second_new, first_new / (jnp.sqrt(second_new) + adam_eps)

    at_q, at_o = cols(k, quarter_q), cols(k, quarter_o)
    normed_q = update(low[:, :quarter_q], fq_ref[:, at_q], sq_ref[:, at_q])[2]
    normed_o = update(low[:, quarter_q:], fo_ref[:, at_o], so_ref[:, at_o])[2]
    half[k, f, :, :quarter_q] = normed_q.astype(BF16)
    half[k, f, :, quarter_q:] = normed_o.astype(BF16)
    share = jnp.sum(normed_q * normed_q) + jnp.sum(normed_o * normed_o)
    tz[f] = jnp.full(tz.shape[1:], share, F32)
    for j in fs_peers:
        sent.append(send(tz.at[f], tz.at[f], tz_s.at[j], tz_r.at[f], {"fs": j}))
        sent.append(send(half.at[k, f], half.at[k, f], hz_s.at[j], hz_r.at[f], {"fs": j}))
    for j in rep_peers:
        sent.append(send(half.at[k, f], half.at[k, f], hr_s.at[f, j], hr_r.at[f, k], {"rep": j}))

    for j in fs_peers:
        arrived(tz.at[j], tz_s.at[j], tz_r.at[j], {"fs": j})
    tr[k] = jnp.sum(tz[...], axis=0)
    for j in rep_peers:
        sent.append(send(tr.at[k], tr.at[k], tr_s.at[j], tr_r.at[k], {"rep": j}))
    for j in fs_peers:
        arrived(half.at[k, j], hz_s.at[j], hz_r.at[j], {"fs": j})
        for m in rep_peers:
            sent.append(send(half.at[k, j], half.at[k, j], hr_s.at[j, m], hr_r.at[j, k], {"rep": m}))
    for j in rep_peers:
        arrived(tr.at[j], tr_s.at[j], tr_r.at[j], {"rep": j})
    tt[t] = jnp.sum(tr[...], axis=0)
    sent.append(send(tt.at[t], tt.at[t], tt_s.at[0], tt_r.at[0], other))

    def weights(index, scale):
        block = half[index].reshape(rank, quarter_q + quarter_o)
        for proj, lo, hi, width, old, new, step, copy, rows in (
            (pq_ref, 0, quarter_q, quarter_q, wq_ref, nwq, stq, cpq, rows_q),
            (po_ref, quarter_q, quarter_q + quarter_o, quarter_o, wo_ref, nwo, sto, cpo, rows_o),
        ):
            at = cols(index, width)
            moved = scale * jnp.dot(proj[...], block[:, lo:hi], preferred_element_type=F32)
            fresh = old[:, at] - learn_rate * moved
            step[:, at] = moved
            new[:, at] = fresh
            copy[cols(f, rows), at] = fresh.astype(BF16)

    arrived(tt.at[1 - t], tt_s.at[0], tt_r.at[0], other)
    scale = lax.rsqrt((tt[0] + tt[1])[:1, :1] / entries + mean_eps)
    weights(k, scale)
    outs = ((cpq, rows_q, quarter_q, 0), (cpo, rows_o, quarter_o, 1))
    for j in fs_peers:
        for copy, rows, width, i in outs:
            block = copy.at[cols(f, rows), cols(k, width)]
            sent.append(send(block, block, cz_s.at[i, j], cz_r.at[i, f], {"fs": j}))
    for j in rep_peers:
        sent.append(send(lowg.at[k], lowg.at[k], lg_s.at[j], lg_r.at[k], {"rep": j}))
    for m in rep_peers:
        for j in [f] + fs_peers:
            arrived(half.at[m, j], hr_s.at[j, m], hr_r.at[j, m], {"rep": m})
        weights(m, scale)
    for j in fs_peers:
        for copy, rows, width, i in outs:
            block = copy.at[cols(j, rows), cols(k, width)]
            arrived(block, cz_s.at[i, j], cz_r.at[i, j], {"fs": j})
            for m in rep_peers:
                sent.append(send(block, block, cr_s.at[i, j, m], cr_r.at[i, j, k], {"rep": m}))
    for m in [k] + rep_peers:
        if m is not k:
            arrived(lowg.at[m], lg_s.at[m], lg_r.at[m], {"rep": m})
        block = lowg[m]
        at_q, at_o = cols(m, quarter_q), cols(m, quarter_o)
        nfq[:, at_q], nsq[:, at_q], _ = update(block[:, :quarter_q], fq_ref[:, at_q], sq_ref[:, at_q])
        nfo[:, at_o], nso[:, at_o], _ = update(block[:, quarter_q:], fo_ref[:, at_o], so_ref[:, at_o])
    for j in fs_peers:
        for m in rep_peers:
            for copy, rows, width, i in outs:
                block = copy.at[cols(j, rows), cols(m, width)]
                arrived(block, cr_s.at[i, j, m], cr_r.at[i, j, m], {"rep": m})
    for copy in sent:
        copy.wait_send()


def solution(mesh):
    n, r, tp = mesh.shape["fs"], mesh.shape["rep"], mesh.shape["tp"]

    def local(*args):
        x, qc, a, oc, pq, po, wq, wo, fq, sq, fo, so = args
        rank = pq.shape[1]
        low_rows = fq.shape[0]
        wide = (fq.shape[1] + fo.shape[1]) // r
        entries = rank * (fq.shape[1] + fo.shape[1]) * tp
        shape = jax.ShapeDtypeStruct
        like = lambda v: shape(v.shape, v.dtype)
        dma = pltpu.SemaphoreType.DMA
        return pl.pallas_call(
            functools.partial(kernel, n, r, tp, entries),
            out_shape=(
                like(wq), like(wo), like(wq), like(wo), like(fq), like(sq), like(fo), like(so),
                shape((n * wq.shape[0], wq.shape[1]), BF16),
                shape((n * wo.shape[0], wo.shape[1]), BF16),
            ),
            in_specs=[pl.BlockSpec(memory_space=pltpu.VMEM)] * 12,
            out_specs=[pl.BlockSpec(memory_space=pltpu.VMEM)] * 10,
            scratch_shapes=[
                pltpu.VMEM((n,) + pq.shape, BF16),
                pltpu.VMEM((n,) + po.shape, BF16),
                pltpu.VMEM((r,) + x.shape, BF16),
                pltpu.VMEM((r,) + a.shape, BF16),
                pltpu.VMEM((r, qc.shape[0], qc.shape[1] // r), BF16),
                pltpu.VMEM((r, oc.shape[0], oc.shape[1] // r), BF16),
                pltpu.VMEM((n, low_rows, wide), F32),
                pltpu.VMEM((n, low_rows, wide), F32),
                pltpu.VMEM((r, low_rows, wide), F32),
                pltpu.VMEM((r, n, low_rows, wide), BF16),
                pltpu.VMEM((n, 8, 128), F32),
                pltpu.VMEM((r, 8, 128), F32),
                pltpu.VMEM((tp, 8, 128), F32),
                dma((2, n)), dma((2, n)), dma((2, n)), dma((2, n)),
                dma((2, r)), dma((2, r)), dma((2, r)), dma((2, r)), dma((2, r)), dma((2, r)), dma((n,)), dma((n,)), dma((r,)), dma((r,)),
                dma((n,)), dma((n,)), dma((n, r)), dma((n, r)),
                dma((n,)), dma((n,)), dma((r,)), dma((r,)), dma((1,)), dma((1,)),
                dma((2, n)), dma((2, n)), dma((2, n, r)), dma((2, n, r)),
            ],
            compiler_params=pltpu.CompilerParams(collective_id=0, has_side_effects=True),
        )(*args)

    both, rows = P(("fs", "rep"), "tp"), P("fs", "tp")
    whole = P(("fs", "rep"), None)
    return jax.shard_map(
        local,
        mesh=mesh,
        in_specs=(whole, both, whole, both, P("fs", None), P("fs", None)) + (rows,) * 6,
        out_specs=(rows,) * 8 + (P(None, "tp"),) * 2,
        check_vma=False,
    )
```

time: 285 us -> 126 us (0.44)
  the two profiles are of different devices: /device:TPU:27 before, /device:TPU:9 now
where the time goes in v1:
time: 126 us
  Pallas kernels  113 us (90%)
  local copies, waits for them, and re-layouts  11.7 us (9%)
    pallas_call x1, Pallas kernels, local(): pl.pallas_call(functools.partial(kernel, n, r, tp, entries), out_shape=(l...  113 us
    unnamed x28, local copies, waits for them, and re-layouts  11.7 us

profile of v1, /device:TPU:9, one launch (start us, length us, event | category | flops | bytes accessed | tf_op | source)
XLA Modules:
  0.0 125.7 jit_solution(14981551227501712470)
XLA Ops:
  0.6 113.3 %shard_map.195 = (f32[512,512]{1,0:T(8,128)}, f32[256,1024]{1,0:T(8,128)}, f32[512,512]{1,0:T(8,128)}, f32[256,1024]{1,0:T(8,128)}, f32[64,512]{1,0:T(8,128)}, /...) custom-call(bf16[128,2048]{1,0:T(8,128)(2,1)} %x_ref.1, ...), custom_call_target="tpu_custom_call" | custom-call | tf_op jit(solution)/shard_map/pallas_call | solution.py:214
  114.0 0.0 copy-start.4
  114.0 0.0 copy-start.3
  114.0 2.4 %copy.32 = f32[512,512]{1,0:T(8,128)} copy(f32[512,512]{1,0:T(8,128)} %get-tuple-element.20) | data formatting | bytes 2097152
  116.4 0.0 copy-done.4
  116.4 0.0 copy-start.2
  116.4 1.0 copy.33
  117.4 0.0 copy-done.3
  117.4 0.0 copy-start.8
  117.4 0.0 copy-start.7
  117.4 0.0 copy-start.6
  117.4 0.0 copy-start.5
  117.4 1.0 copy.34
  118.4 0.0 copy-done.2
  118.4 0.0 copy-start.1
  118.4 1.0 copy.35
  119.3 0.0 copy-done.8
  119.3 0.7 copy.36
  120.0 0.0 copy-done.7
  120.0 0.7 copy.37
  120.7 0.0 copy-done.6
  120.7 0.7 copy.38
  121.4 0.0 copy-done.5
  121.4 0.7 copy.39
  122.1 0.0 copy-done.1
  122.1 0.0 copy-start
  122.1 1.3 %copy.40 = bf16[2048,512]{1,0:T(8,128)(2,1)} copy(bf16[2048,512]{1,0:T(8,128)(2,1)S(1)} %copy-done.1) | data formatting | bytes 4194304
  123.4 1.0 copy-done
  124.4 1.3 %copy.41 = bf16[1024,1024]{1,0:T(8,128)(2,1)} copy(bf16[1024,1024]{1,0:T(8,128)(2,1)S(1)} %copy-done) | data formatting | bytes 4194304
Async XLA Ops:
  114.0 2.4 %copy-start.4 = (f32[256,1024]{1,0:T(8,128)S(1)}, f32[256,1024]{1,0:T(8,128)}, u32[]{:S(2)}) copy-start(f32[256,1024]{1,0:T(8,128)} %get-tuple-element.21) | copy-start | bytes 3145732
  114.0 3.4 %copy-start.3 = (f32[512,512]{1,0:T(8,128)S(1)}, f32[512,512]{1,0:T(8,128)}, u32[]{:S(2)}) copy-start(f32[512,512]{1,0:T(8,128)} %get-tuple-element.22) | copy-start | bytes 3145732
  116.4 2.0 %copy-start.2 = (f32[256,1024]{1,0:T(8,128)S(1)}, f32[256,1024]{1,0:T(8,128)}, u32[]{:S(2)}) copy-start(f32[256,1024]{1,0:T(8,128)} %get-tuple-element.23) | copy-start | bytes 3145732
  117.4 2.0 %copy-start.8 = (f32[64,512]{1,0:T(8,128)S(1)}, f32[64,512]{1,0:T(8,128)}, u32[]{:S(2)}) copy-start(f32[64,512]{1,0:T(8,128)} %get-tuple-element.24) | copy-start | bytes 393220
  117.4 2.6 %copy-start.7 = (f32[64,512]{1,0:T(8,128)S(1)}, f32[64,512]{1,0:T(8,128)}, u32[]{:S(2)}) copy-start(f32[64,512]{1,0:T(8,128)} %get-tuple-element.25) | copy-start | bytes 393220
  117.4 3.3 %copy-start.6 = (f32[64,1024]{1,0:T(8,128)S(1)}, f32[64,1024]{1,0:T(8,128)}, u32[]{:S(2)}) copy-start(f32[64,1024]{1,0:T(8,128)} %get-tuple-element.26) | copy-start | bytes 786436
  117.4 4.0 %copy-start.5 = (f32[64,1024]{1,0:T(8,128)S(1)}, f32[64,1024]{1,0:T(8,128)}, u32[]{:S(2)}) copy-start(f32[64,1024]{1,0:T(8,128)} %get-tuple-element.27) | copy-start | bytes 786436
  118.4 3.7 %copy-start.1 = (bf16[2048,512]{1,0:T(8,128)(2,1)S(1)}, bf16[2048,512]{1,0:T(8,128)(2,1)}, u32[]{:S(2)}) copy-start(bf16[2048,512]{1,0:T(8,128)(2,1)} %get-tuple-element.28) | copy-start | bytes 6291460
  122.1 2.3 %copy-start = (bf16[1024,1024]{1,0:T(8,128)(2,1)S(1)}, bf16[1024,1024]{1,0:T(8,128)(2,1)}, u32[]{:S(2)}) copy-start(bf16[1024,1024]{1,0:T(8,128)(2,1)} %get-tuple-element.29) | copy-start | bytes 6291460

commit v2 on v1

--- a/solution.py
+++ b/solution.py
@@ -34,6 +34,7 @@
     quarter_q, quarter_o = fq_ref.shape[1] // r, fo_ref.shape[1] // r
     fs_peers = [lax.rem(f + d, n) for d in range(1, n)]
     rep_peers = [lax.rem(k + d, r) for d in range(1, r)]
+    from_fs, from_rep = fs_peers[::-1], rep_peers[::-1]
 
     def send(src, dst, ssem, rsem, where):
         copy = pltpu.make_async_remote_copy(
@@ -81,8 +82,8 @@
     alloc[k] = oc_ref[:, cols(k, quarter_o)]
     for d in range(max(n, r) - 1):
         for peers, group, s1, r1, s2, r2_, axis in (
-            (fs_peers, pieces, pz_s, pz_r, pt_s, pt_r, "fs"),
-            (rep_peers, loads, xr_s, xr_r, xt_s, xt_r, "rep"),
+            (from_fs, pieces, pz_s, pz_r, pt_s, pt_r, "fs"),
+            (from_rep, loads, xr_s, xr_r, xt_s, xt_r, "rep"),
         ):
             if d >= len(peers):
                 continue
@@ -141,7 +142,7 @@
     tr[k] = jnp.sum(tz[...], axis=0)
     for j in rep_peers:
         sent.append(send(tr.at[k], tr.at[k], tr_s.at[j], tr_r.at[k], {"rep": j}))
-    for j in fs_peers:
+    for j in from_fs:
         arrived(half.at[k, j], hz_s.at[j], hz_r.at[j], {"fs": j})
         for m in rep_peers:
             sent.append(send(half.at[k, j], half.at[k, j], hr_s.at[j, m], hr_r.at[j, k], {"rep": m}))
@@ -173,16 +174,38 @@
             sent.append(send(block, block, cz_s.at[i, j], cz_r.at[i, f], {"fs": j}))
     for j in rep_peers:
         sent.append(send(lowg.at[k], lowg.at[k], lg_s.at[j], lg_r.at[k], {"rep": j}))
-    for m in rep_peers:
-        for j in [f] + fs_peers:
+    for m in from_rep:
+        for j in [f] + from_fs:
             arrived(half.at[m, j], hr_s.at[j, m], hr_r.at[j, m], {"rep": m})
         weights(m, scale)
-    for j in fs_peers:
-        for copy, rows, width, i in outs:
-            block = copy.at[cols(j, rows), cols(k, width)]
+    across = r == 4
+    if across:
+        near, far = k + 1 - 2 * lax.rem(k, 2), lax.rem(k + 2, r)
+        beyond = lax.rem(near + 2, r)
+        targets = [near, far]
+    else:
+        targets = rep_peers
+
+    def block_of(i, j, m):
+        copy, rows, width, _ = outs[i]
+        return copy.at[cols(j, rows), cols(m, width)]
+
+    def relay(j):
+        for i, source, to in ((0, near, far), (1, far, near)):
+            block = block_of(i, j, source)
+            arrived(block, cr_s.at[i, j, source], cr_r.at[i, j, source], {"rep": source})
+            sent.append(send(block, block, cr_s.at[i, j, beyond], cr_r.at[i, j, source], {"rep": to}))
+
+    for step, j in enumerate(from_fs):
+        for i in range(2):
+            block = block_of(i, j, k)
             arrived(block, cz_s.at[i, j], cz_r.at[i, j], {"fs": j})
-            for m in rep_peers:
+            for m in targets:
                 sent.append(send(block, block, cr_s.at[i, j, m], cr_r.at[i, j, k], {"rep": m}))
+        if across and step:
+            relay(from_fs[step - 1])
+    if across and from_fs:
+        relay(from_fs[-1])
     for m in [k] + rep_peers:
         if m is not k:
             arrived(lowg.at[m], lg_s.at[m], lg_r.at[m], {"rep": m})
@@ -190,13 +213,22 @@
         at_q, at_o = cols(m, quarter_q), cols(m, quarter_o)
         nfq[:, at_q], nsq[:, at_q], _ = update(block[:, :quarter_q], fq_ref[:, at_q], sq_ref[:, at_q])
         nfo[:, at_o], nso[:, at_o], _ = update(block[:, quarter_q:], fo_ref[:, at_o], so_ref[:, at_o])
-    for j in fs_peers:
-        for m in rep_peers:
-            for copy, rows, width, i in outs:
-                block = copy.at[cols(j, rows), cols(m, width)]
-                arrived(block, cr_s.at[i, j, m], cr_r.at[i, j, m], {"rep": m})
+    late = ((1, near), (0, far), (0, beyond), (1, beyond)) if across else [(i, m) for m in from_rep for i in range(2)]
+    for j in from_fs:
+        for i, m in late:
+            arrived(block_of(i, j, m), cr_s.at[i, j, m], cr_r.at[i, j, m], {"rep": m})
     for copy in sent:
         copy.wait_send()
+
+
+def place(*refs):
+    count = len(refs) // 2
+    sems = refs[-1]
+    copies = [pltpu.make_async_copy(refs[i], refs[count + i], sems.at[i]) for i in range(count)]
+    for copy in copies:
+        copy.start()
+    for copy in copies:
+        copy.wait()
 
 
 def solution(mesh):
@@ -211,7 +243,7 @@
         shape = jax.ShapeDtypeStruct
         like = lambda v: shape(v.shape, v.dtype)
         dma = pltpu.SemaphoreType.DMA
-        return pl.pallas_call(
+        made = pl.pallas_call(
             functools.partial(kernel, n, r, tp, entries),
             out_shape=(
                 like(wq), like(wo), like(wq), like(wo), like(fq), like(sq), like(fo), like(so),
@@ -242,6 +274,13 @@
             ],
             compiler_params=pltpu.CompilerParams(collective_id=0, has_side_effects=True),
         )(*args)
+        return pl.pallas_call(
+            place,
+            out_shape=tuple(like(v) for v in made),
+            in_specs=[pl.BlockSpec(memory_space=pltpu.VMEM)] * len(made),
+            out_specs=[pl.BlockSpec(memory_space=pl.ANY)] * len(made),
+            scratch_shapes=[dma((len(made),))],
+        )(*made)
 
     both, rows = P(("fs", "rep"), "tp"), P("fs", "tp")
     whole = P(("fs", "rep"), None)

time: 126 us -> 106 us (0.84)
  the two profiles are of different devices: /device:TPU:9 before, /device:TPU:27 now
where the time goes in v2:
time: 106 us
  Pallas kernels  105 us (99%)
    pallas_call x1, Pallas kernels, local(): pl.pallas_call(functools.partial(kernel, n, r, tp, entries), out_shape=(l...  97.7 us
    pallas_call x1, Pallas kernels, local(): pl.pallas_call(place, out_shape=tuple((like(v) for v in made)), in_specs=...  7.37 us

profile of v2, /device:TPU:27, one launch (start us, length us, event | category | flops | bytes accessed | tf_op | source)
XLA Modules:
  0.0 105.8 jit_solution(11327782133850250766)
XLA Ops:
  0.6 97.7 %shard_map.195 = (f32[512,512]{1,0:T(8,128)}, f32[256,1024]{1,0:T(8,128)}, f32[512,512]{1,0:T(8,128)}, f32[256,1024]{1,0:T(8,128)}, f32[64,512]{1,0:T(8,128)}, /...) custom-call(bf16[128,2048]{1,0:T(8,128)(2,1)} %x_ref.1, ...), custom_call_target="tpu_custom_call" | custom-call | tf_op jit(solution)/shard_map/pallas_call | solution.py:246
  98.4 7.4 %shard_map.196 = (f32[512,512]{1,0:T(8,128)}, f32[256,1024]{1,0:T(8,128)}, f32[512,512]{1,0:T(8,128)}, f32[256,1024]{1,0:T(8,128)}, f32[64,512]{1,0:T(8,128)}, /...) custom-call(f32[512,512]{1,0:T(8,128)} %get-tuple-element.20.refs_0_, ...), custom_call_target="tpu_custom_call" | custom-call | tf_op jit(solution)/shard_map/pallas_call | solution.py:277

commit v3 on v2

--- a/solution.py
+++ b/solution.py
@@ -35,6 +35,13 @@
     fs_peers = [lax.rem(f + d, n) for d in range(1, n)]
     rep_peers = [lax.rem(k + d, r) for d in range(1, r)]
     from_fs, from_rep = fs_peers[::-1], rep_peers[::-1]
+    across = r == 4
+    if across:
+        near, far = k + 1 - 2 * lax.rem(k, 2), lax.rem(k + 2, r)
+        beyond = lax.rem(near + 2, r)
+        targets = [near, far]
+    else:
+        targets = rep_peers
 
     def send(src, dst, ssem, rsem, where):
         copy = pltpu.make_async_remote_copy(
@@ -67,7 +74,7 @@
         for own, whole, part, i in pieces:
             mine = cols(t, part)
             sent.append(send(own.at[mine], whole.at[f, mine], pz_s.at[i, j], pz_r.at[i, f], {"fs": j}))
-    for j in rep_peers:
+    for j in targets:
         for own, whole, part, i in loads:
             mine = cols(t, part)
             sent.append(send(own.at[mine], whole.at[k, mine], xr_s.at[i, j], xr_r.at[i, k], {"rep": j}))
@@ -80,22 +87,47 @@
     alla[k] = a_ref[...]
     allqc[k] = qc_ref[:, cols(k, quarter_q)]
     alloc[k] = oc_ref[:, cols(k, quarter_o)]
-    for d in range(max(n, r) - 1):
-        for peers, group, s1, r1, s2, r2_, axis in (
-            (from_fs, pieces, pz_s, pz_r, pt_s, pt_r, "fs"),
-            (from_rep, loads, xr_s, xr_r, xt_s, xt_r, "rep"),
-        ):
-            if d >= len(peers):
-                continue
-            j = peers[d]
-            for own, whole, part, i in group:
-                mine = cols(t, part)
-                arrived(whole.at[j, mine], s1.at[i, j], r1.at[i, j], {axis: j})
-                sent.append(send(whole.at[j, mine], whole.at[j, mine], s2.at[i, j], r2_.at[i, j], other))
-    for peers, group, s2, r2_ in ((fs_peers, pieces, pt_s, pt_r), (rep_peers, loads, xt_s, xt_r)):
+    def hand_over(group, j, s1, r1, s2, r2_, axis):
+        for own, whole, part, i in group:
+            mine = cols(t, part)
+            arrived(whole.at[j, mine], s1.at[i, j], r1.at[i, j], {axis: j})
+            sent.append(send(whole.at[j, mine], whole.at[j, mine], s2.at[i, j], r2_.at[i, j], other))
+
+    def half_rows(part, which):
+        return cols(2 * t + which, part // 2)
+
+    def pass_on(source, to, which):
+        for own, whole, part, i in loads:
+            rows = half_rows(part, which)
+            block = whole.at[source, rows]
+            sent.append(send(block, block, xr_s.at[i + 2 * which, beyond], xr_r.at[i + 2 * which, source], {"rep": to}))
+
+    if across:
+        for which, (source, to) in enumerate(((near, far), (far, near))):
+            hand_over(loads, source, xr_s, xr_r, xt_s, xt_r, "rep")
+            pass_on(source, to, which)
+    else:
+        for j in from_rep:
+            hand_over(loads, j, xr_s, xr_r, xt_s, xt_r, "rep")
+    for j in from_fs:
+        hand_over(pieces, j, pz_s, pz_r, pt_s, pt_r, "fs")
+    if across:
+        for own, whole, part, i in loads:
+            for which in range(2):
+                block = whole.at[beyond, half_rows(part, which)]
+                at = i + 2 * which
+                arrived(block, xr_s.at[at, beyond], xr_r.at[at, beyond], {"rep": beyond})
+                sent.append(send(block, block, xt_s.at[at, beyond], xt_r.at[at, beyond], other))
+    for peers, group, s2, r2_ in ((fs_peers, pieces, pt_s, pt_r), (targets, loads, xt_s, xt_r)):
         for j in peers:
             for own, whole, part, i in group:
                 arrived(whole.at[j, cols(1 - t, part)], s2.at[i, j], r2_.at[i, j], other)
+    if across:
+        for own, whole, part, i in loads:
+            for which in range(2):
+                block = whole.at[beyond, cols(2 * (1 - t) + which, part // 2)]
+                at = i + 2 * which
+                arrived(block, xt_s.at[at, beyond], xt_r.at[at, beyond], other)
     for j in rep_peers:
         for whole, i in ((allqc, 0), (alloc, 1)):
             arrived(whole.at[j], cr1_s.at[i, j], cr1_r.at[i, j], {"rep": j})
@@ -178,14 +210,6 @@
         for j in [f] + from_fs:
             arrived(half.at[m, j], hr_s.at[j, m], hr_r.at[j, m], {"rep": m})
         weights(m, scale)
-    across = r == 4
-    if across:
-        near, far = k + 1 - 2 * lax.rem(k, 2), lax.rem(k + 2, r)
-        beyond = lax.rem(near + 2, r)
-        targets = [near, far]
-    else:
-        targets = rep_peers
-
     def block_of(i, j, m):
         copy, rows, width, _ = outs[i]
         return copy.at[cols(j, rows), cols(m, width)]
@@ -267,7 +291,7 @@
                 pltpu.VMEM((r, 8, 128), F32),
                 pltpu.VMEM((tp, 8, 128), F32),
                 dma((2, n)), dma((2, n)), dma((2, n)), dma((2, n)),
-                dma((2, r)), dma((2, r)), dma((2, r)), dma((2, r)), dma((2, r)), dma((2, r)), dma((n,)), dma((n,)), dma((r,)), dma((r,)),
+                dma((4, r)), dma((4, r)), dma((4, r)), dma((4, r)), dma((2, r)), dma((2, r)), dma((n,)), dma((n,)), dma((r,)), dma((r,)),
                 dma((n,)), dma((n,)), dma((n, r)), dma((n, r)),
                 dma((n,)), dma((n,)), dma((r,)), dma((r,)), dma((1,)), dma((1,)),
                 dma((2, n)), dma((2, n)), dma((2, n, r)), dma((2, n, r)),

time: 106 us -> 104 us (0.981)
  Pallas kernels: 105 us -> 103 us
    pallas_call x1, Pallas kernels: 97.7 us -> 95.2 us  [local(): pl.pallas_call(functools.partial(kernel, n, r, tp, entries), out_shape=(l...]
where the time goes in v3:
time: 104 us; the launch traced here: 103 us
  Pallas kernels  103 us (99%)
    pallas_call x1, Pallas kernels, local(): pl.pallas_call(functools.partial(kernel, n, r, tp, entries), out_shape=(l...  95.2 us
    pallas_call x1, Pallas kernels, local(): pl.pallas_call(place, out_shape=tuple((like(v) for v in made)), in_specs=...  7.37 us

profile of v3, /device:TPU:27, one launch (start us, length us, event | category | flops | bytes accessed | tf_op | source)
XLA Modules:
  0.0 103.3 jit_solution(13585069492952552160)
XLA Ops:
  0.6 95.2 %shard_map.195 = (f32[512,512]{1,0:T(8,128)}, f32[256,1024]{1,0:T(8,128)}, f32[512,512]{1,0:T(8,128)}, f32[256,1024]{1,0:T(8,128)}, f32[64,512]{1,0:T(8,128)}, /...) custom-call(bf16[128,2048]{1,0:T(8,128)(2,1)} %x_ref.1, ...), custom_call_target="tpu_custom_call" | custom-call | tf_op jit(solution)/shard_map/pallas_call | solution.py:270
  95.9 7.4 %shard_map.196 = (f32[512,512]{1,0:T(8,128)}, f32[256,1024]{1,0:T(8,128)}, f32[512,512]{1,0:T(8,128)}, f32[256,1024]{1,0:T(8,128)}, f32[64,512]{1,0:T(8,128)}, /...) custom-call(f32[512,512]{1,0:T(8,128)} %get-tuple-element.20.refs_0_, ...), custom_call_target="tpu_custom_call" | custom-call | tf_op jit(solution)/shard_map/pallas_call | solution.py:301
